TPU v7x, 32 devices: a whole 2x2x4 slice. The times are simulated.
32 devices in a mesh: grp: 2 (over y), sp: 4 (over z), tp: 4 (over x, core).
Axes of the slice: x: 2, y: 2, z: 4, core: 2. Of those that a mesh axis runs over, the one named last changes fastest.
Arguments:
- tokens: bfloat16 [1024, 2048], P(('grp', 'sp')), parts along dimension 0, may hold values from -6 to 6
- norm_gain: float32 [2048], replicated, may hold values from 0.1 to 1.9
- w_query: bfloat16 [2048, 512], P('sp', 'tp'), may hold values from -0.125 to 0.125
- w_key: bfloat16 [2048, 512], P('sp', 'tp'), may hold values from -0.125 to 0.125
- w_value: bfloat16 [2048, 512], P('sp', 'tp'), may hold values from -0.125 to 0.125
- w_glu_value: bfloat16 [2048, 1024], P('sp', 'tp'), may hold values from -0.125 to 0.125
- w_glu_gate: bfloat16 [2048, 1024], P('sp', 'tp'), may hold values from -0.125 to 0.125
- key_offset: bfloat16 [1024, 8], P(('grp', 'sp'), 'tp'), parts along dimension 0, may hold values from -13 to 0
- head_gain: float32 [8, 64], P('tp'), may hold values from 0.1 to 1.9
- conv_taps: float32 [31, 1024], P(None, 'tp'), may hold values from -2.873685 to 2.873685
- channel_gain: float32 [1024], P('tp'), may hold values from 0.1 to 1.9
- channel_bias: float32 [1024], P('tp'), may hold values from -3 to 3
- w_out_attn: bfloat16 [512, 2048], P('tp'), may hold values from -0.15625 to 0.15625
- w_out_conv: bfloat16 [1024, 2048], P('tp'), may hold values from -0.15625 to 0.15625
- out_gain: float32 [2048], replicated, may hold values from 0.1 to 1.9
Outputs:
- mixed: bfloat16 [1024, 2048], P(('grp', 'sp')), parts along dimension 0
- log_mass: float32 [8, 1024], P('tp', ('grp', 'sp')), parts along dimension 1
There are 2 independent parts, one for each index of `grp`. A program takes and returns all parts, laid end to end along the dimension named above; an argument that names none is the same for every part. Nothing has to cross between parts.
All inputs are finite; a program needn't handle non-finite values.
Results may differ from a plain program's by a relative error of at most 0.011.
Values may be sent and summed in bfloat16 or wider, within the bound.
No kernel may reach another device: no remote copies, remote signals or barrier semaphores. Data moves between devices by JAX's collectives and lax.ppermute only.
A program may use at most 64 MiB of HBM per device.

v0:
```python
import jax
import jax.numpy as jnp
from jax import lax
from jax.sharding import PartitionSpec as P

HD = 64
CW = 1024
norm_eps = 1e-06


def from_behind(value, axis, steps):
    count = lax.axis_size(axis)
    initial, last = (max(0, -steps), min(count, count - steps))
    return lax.ppermute(value, axis, [(source, source + steps) for source in range(initial, last)])


def row_norm(values_in, gain_vec):
    squares = jnp.mean(values_in * values_in, axis=-1, keepdims=True)
    return values_in * lax.rsqrt(squares + norm_eps) * gain_vec


def local(
    tokens,
    norm_gain,
    w_query,
    w_key,
    w_value,
    w_glu_value,
    w_glu_gate,
    key_offset,
    head_gain,
    conv_taps,
    channel_gain,
    channel_bias,
    w_out_attn,
    w_out_conv,
    out_gain,
):
    row_count = tokens.shape[0]
    normed = row_norm(tokens.astype(jnp.float32), norm_gain).astype(jnp.bfloat16)
    weights_in = (w_query, w_key, w_value, w_glu_value, w_glu_gate)
    pieces = (
        lax.all_gather(weights_in[0], "sp", axis=0, tiled=True),
        lax.all_gather(weights_in[1], "sp", axis=0, tiled=True),
        lax.all_gather(weights_in[2], "sp", axis=0, tiled=True),
        lax.all_gather(weights_in[3], "sp", axis=0, tiled=True),
        lax.all_gather(weights_in[4], "sp", axis=0, tiled=True),
    )
    projected = tuple(
        (jnp.dot(normed, shard_piece, preferred_element_type=jnp.float32) for shard_piece in pieces)
    )
    query, key_rows, value_rows, glu_value, glu_gate = [
        summed.astype(jnp.bfloat16) for summed in projected
    ]
    kv_local = key_rows.shape[1] // HD
    group_size = query.shape[1] // key_rows.shape[1]
    heads_local = kv_local * group_size
    all_keys, all_values, all_offsets = (
        lax.all_gather(key_rows, "sp", axis=0, tiled=True),
        lax.all_gather(value_rows, "sp", axis=0, tiled=True),
        lax.all_gather(key_offset, "sp", axis=0, tiled=True),
    )
    sequence_length_total = all_keys.shape[0]
    shard_count = lax.axis_size("sp")
    per_block = 1
    while (
        per_block * 2 <= shard_count
        and shard_count % (per_block * 2) == 0
        and (per_block * 2 * row_count <= 1024)
    ):
        per_block = per_block * 2
    span_len = per_block * row_count
    query_heads = query.reshape(row_count, kv_local, group_size, HD)
    key_heads = all_keys.reshape(sequence_length_total, kv_local, HD)
    value_heads = all_values.reshape(sequence_length_total, kv_local, HD)
    my_index = lax.axis_index("sp")
    query_pos = my_index * row_count + jnp.arange(row_count, dtype=jnp.int32)
    last_block = my_index // per_block
    zeros_mix = jnp.zeros((kv_local, group_size, row_count, HD), jnp.float32)
    zeros_row = jnp.zeros((kv_local, group_size, row_count), jnp.float32)

    def sweep(turn_index, carry):
        head_mix, mass_sum, carried = carry
        first_key = (last_block - turn_index) * span_len
        key_block = lax.dynamic_slice_in_dim(key_heads, first_key, span_len, 0)
        value_block = lax.dynamic_slice_in_dim(value_heads, first_key, span_len, 0)
        offset_block = lax.dynamic_slice_in_dim(all_offsets, first_key, span_len, 0).astype(
            jnp.float32
        )
        offset_block = offset_block.T.reshape(kv_local, group_size, 1, span_len)
        scores = (
            jnp.einsum("qhgd,khd->hgqk", query_heads, key_block, preferred_element_type=jnp.float32)
            * HD ** (-0.5)
            + offset_block
        )
        key_pos = first_key + jnp.arange(span_len, dtype=jnp.int32)
        allowed = key_pos[None, :] <= query_pos[:, None]
        log_not = jnp.where(allowed, jax.nn.log_sigmoid(-scores), 0.0)
        later = lax.cumsum(log_not, axis=3, reverse=True) - log_not + carried[..., None]
        weights = jnp.where(allowed, jnp.exp(jax.nn.log_sigmoid(scores) + later), 0.0)
        head_mix = head_mix + jnp.einsum(
            "hgqk,khd->hgqd",
            weights.astype(jnp.bfloat16),
            value_block,
            preferred_element_type=jnp.float32,
        )
        return (head_mix, mass_sum + jnp.sum(weights, axis=3), carried + jnp.sum(log_not, axis=3))

    head_mix, mass_sum, leftover = lax.fori_loop(
        0, last_block + 1, sweep, (zeros_mix, zeros_row, zeros_row)
    )
    log_mass = jnp.log(mass_sum).reshape(heads_local, row_count)
    head_rows = head_mix.transpose(2, 0, 1, 3).reshape(row_count, heads_local, HD)
    attended = (
        row_norm(head_rows, head_gain).astype(jnp.bfloat16).reshape(row_count, heads_local * HD)
    )
    gated = (glu_value.astype(jnp.float32) * jax.nn.sigmoid(glu_gate.astype(jnp.float32))).astype(
        jnp.bfloat16
    )
    reach_len = conv_taps.shape[0] - 1
    before = from_behind(gated[row_count - reach_len :], "sp", 1)
    padded = jnp.concatenate([before, gated], axis=0).astype(jnp.float32)
    conv_out = jnp.zeros(gated.shape, jnp.float32)
    for tap_index in range(conv_taps.shape[0]):
        conv_out = conv_out + conv_taps[tap_index] * padded[tap_index : tap_index + row_count]
    total_sum, total_squares = lax.psum(
        (jnp.sum(conv_out, axis=1), jnp.sum(conv_out * conv_out, axis=1)), "tp"
    )
    chan_mean = (total_sum / CW)[:, None]
    spread = (total_squares / CW)[:, None] - chan_mean * chan_mean
    centered = conv_out - chan_mean
    channel_out = jax.nn.silu(
        centered * lax.rsqrt(spread + norm_eps) * channel_gain + channel_bias
    ).astype(jnp.bfloat16)
    share = lax.psum_scatter(
        jnp.dot(attended, w_out_attn, preferred_element_type=jnp.float32)
        + jnp.dot(channel_out, w_out_conv, preferred_element_type=jnp.float32),
        "tp",
        scatter_dimension=0,
        tiled=True,
    )
    mixed = lax.all_gather(row_norm(share, out_gain).astype(jnp.bfloat16), "tp", axis=0, tiled=True)
    return (mixed, log_mass)


def solution(mesh):
    in_specs = (
        P(("grp", "sp"), None),
        P(),
        P("sp", "tp"),
        P("sp", "tp"),
        P("sp", "tp"),
        P("sp", "tp"),
        P("sp", "tp"),
        P(("grp", "sp"), "tp"),
        P("tp", None),
        P(None, "tp"),
        P("tp"),
        P("tp"),
        P("tp", None),
        P("tp", None),
        P(),
    )
    out_specs = (P(("grp", "sp"), None), P("tp", ("grp", "sp")))
    return jax.shard_map(local, mesh=mesh, in_specs=in_specs, out_specs=out_specs, check_vma=False)
```

profile of v0, /device:TPU:0, one launch (start us, length us, event | category | flops | bytes accessed | tf_op | source)
XLA Modules:
  0.0 168.1 jit_solution(18097645065637768242)
XLA Ops:
  7.2 0.0 all-gather.3.cloned.1.call-start
  7.2 0.7 all-gather.3.cloned.1.call-update
  7.9 0.0 all-gather.5.cloned.1.call-start
  8.0 0.7 all-gather.5.cloned.1.call-update
  8.7 0.0 reduce-scatter.2.cloned.1.call-start
  8.8 0.2 fusion.28
  9.0 0.7 copy-done.4
  9.7 21.4 %all_gather.28 = bf16[2048,128]{1,0:T(8,128)(2,1)S(1)} all-gather(bf16[512,128]{1,0:T(8,128)(2,1)S(1)} %copy-done.4), channel_id=1, replica_groups=mesh['grp'=2,'sp'=4,'tp'=4] {'sp'}, dimensions={0}, use_global_device_ids=true | all-gather | bytes 655360 | tf_op jit(solution)/shard_map/all_gather | solution.py:44
  31.1 0.4 convolution_convert_fusion.3
  31.4 14.8 %all_gather.29 = bf16[512,128]{1,0:T(8,128)(2,1)S(1)} all-gather(bf16[128,128]{1,0:T(8,128)(2,1)S(1)} %convolution_convert_fusion.3), channel_id=1, replica_groups=mesh['grp'=2,'sp'=4,'tp'=4] {'sp'}, dimensions={0}, use_global_device_ids=true | all-gather | bytes 163840 | tf_op jit(solution)/shard_map/all_gather | solution.py:59
  46.2 0.1 copy.27
  46.4 0.8 copy-done.5
  47.2 18.3 %all_gather.31 = bf16[2048,128]{1,0:T(8,128)(2,1)S(1)} all-gather(bf16[512,128]{1,0:T(8,128)(2,1)S(1)} %copy-done.5), channel_id=1, replica_groups=mesh['grp'=2,'sp'=4,'tp'=4] {'sp'}, dimensions={0}, use_global_device_ids=true | all-gather | bytes 655360 | tf_op jit(solution)/shard_map/all_gather | solution.py:45
  65.5 0.4 convolution_convert_fusion.2
  65.8 15.0 %all_gather.32 = bf16[512,128]{1,0:T(8,128)(2,1)S(1)} all-gather(bf16[128,128]{1,0:T(8,128)(2,1)S(1)} %convolution_convert_fusion.2), channel_id=1, replica_groups=mesh['grp'=2,'sp'=4,'tp'=4] {'sp'}, dimensions={0}, use_global_device_ids=true | all-gather | bytes 163840 | tf_op jit(solution)/shard_map/all_gather | solution.py:60
  80.8 0.1 copy.28
  81.0 0.8 copy-done.6
  81.8 14.7 %all_gather.27 = bf16[2048,128]{1,0:T(8,128)(2,1)S(1)} all-gather(bf16[512,128]{1,0:T(8,128)(2,1)S(1)} %copy-done.6), channel_id=1, replica_groups=mesh['grp'=2,'sp'=4,'tp'=4] {'sp'}, dimensions={0}, use_global_device_ids=true | all-gather | bytes 655360 | tf_op jit(solution)/shard_map/all_gather | solution.py:43
  96.4 0.4 convolution_convert_fusion.4
  96.9 0.6 copy-done.11
  97.5 9.8 %all_gather.30 = bf16[512,2]{0,1:T(2,128)(2,1)S(1)} all-gather(bf16[128,2]{0,1:T(2,128)(2,1)S(1)} %copy-done.11), channel_id=1, replica_groups=mesh['grp'=2,'sp'=4,'tp'=4] {'sp'}, dimensions={0}, use_global_device_ids=true | all-gather | bytes 2560 | tf_op jit(solution)/shard_map/all_gather | solution.py:61
  107.3 4.3 %while.15 = (s32[]{:T(128)}, f32[2,1,128,64]{2,3,0,1:T(8,128)S(1)}, f32[2,1,128]{2,1,0:T(1,128)S(1)}, f32[2,1,128]{2,0,1:T(2,128)S(1)}, s32[]{:T(128)}, /*index=...) while((s32[]{:T(128)}, f32[2,1,128,64]{2,3,0,1:T(8,128)S(1)}, ...), condition=%wide.region_6.7_spmd.clone, body=%wide.region_1.6_spmd.clone.sunk | while | flops 54744452 | bytes 5395625 | solution.py:109
  107.3 0.1 broadcast_compare_fusion.2
  107.4 0.6 fusion.104
  108.0 2.4 %fusion.105 = f32[2,1,128,4,128]{2,3,4,1,0:T(4,128)S(1)} fusion(f32[2,1,128,4,128]{2,4,3,0,1:T(8,128)S(1)} %bitcast.128), kind=kOutput, calls=%fused_computation.18.clone.1 | output fusion | flops 16646144 | bytes 1048576 | tf_op jit(solution)/shard_map/reduce-window
  110.5 0.8 fusion.106
  111.3 0.2 fusion.107
  111.6 0.7 copy-done.7
  112.3 0.0 all-gather.3.cloned.1.call-done
  112.3 1.6 fusion.27
  113.9 0.0 all-gather.5.cloned.1.call-done
  114.0 1.6 fusion.26
  115.6 1.7 %collective-permute-start = (bf16[30,256]{1,0:T(8,128)(2,1)S(1)}, bf16[30,256]{1,0:T(8,128)(2,1)S(1)}, u32[]{:S(2)}, u32[]{:S(2)}) collective-permute-start(bf16[30,256]{1,0:T(8,128)(2,1)S(1)} %slice.262), channel_id=1, source_target_pairs={{0,4},{4,8},{8,12},{1,5},{5,9},{9,13},{2,6},{6,10},{10,14},{3,7},{... | collective-permute-start | bytes 46088 | tf_op jit(solution)/shard_map/ppermute | solution.py:14
  117.3 0.1 mul.427
  117.4 0.1 fusion.63
  117.5 1.2 collective-permute-done
  118.8 0.6 fusion.76
  119.4 5.7 %all-reduce = (f32[128]{0:T(128)S(1)}, f32[128]{0:T(128)S(1)}) all-reduce(f32[128]{0:T(128)S(1)} %get-tuple-element.112, f32[128]{0:T(128)S(1)} %get-tuple-element.111), channel_id=1, replica_groups=mesh['grp'=2,'sp'=4,'tp'=4] {'tp'}, use_global_device_ids=true, to_apply=%region_11.12 | all-reduce | flops 256 | bytes 2048 | tf_op jit(solution)/shard_map/psum | solution.py:126
  125.0 0.7 copy-done.9
  125.7 0.4 fusion.61
  126.1 0.7 copy-done.3
  126.8 1.3 convolution_add_fusion
  128.1 0.6 log_bitcast_fusion
  128.7 24.2 %reduce-scatter.2.cloned.1.call-done = f32[32,2048]{1,0:T(8,128)} async-done(((f32[128,2048]{1,0:T(8,128)}), f32[32,2048]{1,0:T(8,128)}) %reduce-scatter.2.cloned.1.call-update) | async-done | bytes 262160 | tf_op jit(solution)/shard_map/reduce_scatter | solution.py:135
  152.9 1.1 multiply_reduce_fusion
  154.0 0.1 multiply_convert_fusion
  154.1 6.6 %all_gather.35 = bf16[128,2048]{1,0:T(8,128)(2,1)S(1)} all-gather(bf16[32,2048]{1,0:T(8,128)(2,1)S(1)} %multiply_convert_fusion), channel_id=1, replica_groups=mesh['grp'=2,'sp'=4,'tp'=4] {'tp'}, dimensions={0}, use_global_device_ids=true | all-gather | bytes 655360 | tf_op jit(solution)/shard_map/all_gather | solution.py:142
  160.7 0.8 copy.53
  (43 shorter events, 0.3 us)
Async XLA Ops:
  7.2 117.9 %copy-start = (bf16[256,2048]{1,0:T(8,128)(2,1)S(1)}, bf16[256,2048]{1,0:T(8,128)(2,1)}, u32[]{:S(2)}) copy-start(bf16[256,2048]{1,0:T(8,128)(2,1)} %param.30) | copy-start | bytes 3145732
  7.2 1.6 copy-start.2
  7.2 105.2 %all-gather.3.cloned.1.call-start = ((), (), s32[]{:S(2)}) async-start(), calls=%async_computation.1 | async-start | bytes 1310720 | tf_op jit(solution)/shard_map/all_gather | solution.py:46
  7.9 106.0 %all-gather.5.cloned.1.call-start = ((), (), s32[]{:S(2)}) async-start(), calls=%async_computation.2 | async-start | bytes 1310720 | tf_op jit(solution)/shard_map/all_gather | solution.py:47
  8.7 144.2 %reduce-scatter.2.cloned.1.call-start = ((), (), s32[]{:S(2)}) async-start(), calls=%async_computation.3 | async-start | bytes 1310720 | tf_op jit(solution)/shard_map/reduce_scatter | solution.py:135
  8.7 0.9 copy-start.4
  9.7 21.4 %copy-start.12 = (f32[2048]{0:T(1024)S(1)}, f32[2048]{0:T(1024)}, u32[]{:S(2)}) copy-start(f32[2048]{0:T(1024)} %param.18) | copy-start | bytes 24580
  46.2 0.9 copy-start.5
  80.8 0.9 copy-start.6
  96.8 0.7 copy-start.11
  111.5 0.8 copy-start.7
  115.6 1.8 %copy-start.13 = (f32[2,64]{1,0:T(2,128)S(1)}, f32[2,64]{1,0:T(2,128)}, u32[]{:S(2)}) copy-start(f32[2,64]{1,0:T(2,128)} %param.25) | copy-start | bytes 1540
  115.6 3.2 %collective-permute-start = (bf16[30,256]{1,0:T(8,128)(2,1)S(1)}, bf16[30,256]{1,0:T(8,128)(2,1)S(1)}, u32[]{:S(2)}, u32[]{:S(2)}) collective-permute-start(bf16[30,256]{1,0:T(8,128)(2,1)S(1)} %slice.262), channel_id=1, source_target_pairs={{0,4},{4,8},{8,12},{1,5},{5,9},{9,13},{2,6},{6,10},{10,14},{3,7},{... | collective-permute-start | bytes 46088 | tf_op jit(solution)/shard_map/ppermute | solution.py:14
  118.8 6.3 %copy-start.10 = (f32[256]{0:T(256)S(1)}, f32[256]{0:T(256)}, u32[]{:S(2)}) copy-start(f32[256]{0:T(256)} %param.27) | copy-start | bytes 3076
  125.0 0.7 copy-start.9
  125.7 1.0 copy-start.3
  128.1 26.0 %copy-start.8 = (f32[2048]{0:T(1024)S(1)}, f32[2048]{0:T(1024)}, u32[]{:S(2)}) copy-start(f32[2048]{0:T(1024)} %param.31) | copy-start | bytes 24580
  152.9 1.2 copy-start.1
Sparse Core Ops, SparseCore 0:
  9.6 35.8 all-gather.2
  47.1 34.8 all-gather.4
  128.2 24.6 reduce-scatter.1
where the time goes:
time: 169 us; the launch traced here: 168 us
  blocking collectives  106 us (63%)
  waiting for transfers between devices  26.9 us (16%)
  between operations  14 us (8%)
  local copies, waits for them, and re-layouts  6.76 us (4%)
  matrix products  6.76 us (4%)
  other arithmetic  5.54 us (3%)
  starting transfers between devices  1.83 us (1%)
    reduce_scatter x1, waiting for transfers between devices, local(): lax.psum_scatter(jnp.dot(attended, w_out_attn, preferred_element_type=jnp...  24.2 us
    all_gather x1, blocking collectives, local(): lax.all_gather(weights_in[1], 'sp', axis=0, tiled=True)  21.4 us
    all_gather x1, blocking collectives, local(): lax.all_gather(weights_in[2], 'sp', axis=0, tiled=True)  18.3 us
    all_gather x1, blocking collectives, local(): lax.all_gather(value_rows, 'sp', axis=0, tiled=True)  15 us
    all_gather x1, blocking collectives, local(): lax.all_gather(key_rows, 'sp', axis=0, tiled=True)  14.8 us
    all_gather x1, blocking collectives, local(): lax.all_gather(weights_in[0], 'sp', axis=0, tiled=True)  14.7 us
    all_gather x1, blocking collectives, local(): lax.all_gather(key_offset, 'sp', axis=0, tiled=True)  9.75 us
    all_gather x1, blocking collectives, local(): lax.all_gather(row_norm(share, out_gain).astype(jnp.bfloat16), 'tp', axis...  6.6 us
  transfers between devices with their start and end apart: 4, of which 2 were waited for; matrix products, arithmetic and copies ran while one was open for 5% of the time, Pallas kernels for 0%

commit v1 on v0

--- a/solution.py
+++ b/solution.py
@@ -6,6 +6,13 @@
 HD = 64
 CW = 1024
 norm_eps = 1e-06
+
+
+def swapped_in(x, axis, dim):
+    size = lax.axis_size(axis)
+    shards = jnp.stack([x for _ in range(size)])
+    shards = lax.all_to_all(shards, axis, split_axis=0, concat_axis=0)
+    return jnp.concatenate(shards, axis=dim)
 
 
 def from_behind(value, axis, steps):
@@ -41,7 +48,7 @@
     weights_in = (w_query, w_key, w_value, w_glu_value, w_glu_gate)
     pieces = (
         lax.all_gather(weights_in[0], "sp", axis=0, tiled=True),
-        lax.all_gather(weights_in[1], "sp", axis=0, tiled=True),
+        swapped_in(weights_in[1], "sp", 0),
         lax.all_gather(weights_in[2], "sp", axis=0, tiled=True),
         lax.all_gather(weights_in[3], "sp", axis=0, tiled=True),
         lax.all_gather(weights_in[4], "sp", axis=0, tiled=True),

time: 169 us -> 177 us (1.047)
  starting transfers between devices: 1.83 us -> 7.85 us
  blocking collectives: 106 us -> 108 us
    all_gather x1 -> x0, blocking collectives: 21.4 us -> none  [local(): lax.all_gather(weights_in[1], 'sp', axis=0, tiled=True)]
    all_gather x1, blocking collectives: 18.3 us -> 39.7 us  [local(): lax.all_gather(weights_in[2], 'sp', axis=0, tiled=True)]
    all_to_all x0 -> x1, starting transfers between devices: none -> 6.48 us  [swapped_in(): shards = lax.all_to_all(shards, axis, split_axis=0, concat_axis=0)]
    all_gather x1, blocking collectives: 14.7 us -> 18.7 us  [local(): lax.all_gather(weights_in[0], 'sp', axis=0, tiled=True)]
  transfers between devices with their start and end apart: 4 -> 5, of which waited for: 2 -> 2; matrix products, arithmetic and copies ran while one was open for 5% -> 5% of each run, Pallas kernels for 0% -> 0%
where the time goes in v1:
time: 177 us
  blocking collectives  108 us (61%)
  waiting for transfers between devices  27.3 us (15%)
  between operations  14 us (8%)
  starting transfers between devices  7.85 us (4%)
  matrix products  6.74 us (4%)
  local copies, waits for them, and re-layouts  6.68 us (4%)
  other arithmetic  5.53 us (3%)
    all_gather x1, blocking collectives, local(): lax.all_gather(weights_in[2], 'sp', axis=0, tiled=True)  39.7 us
    reduce_scatter x1, waiting for transfers between devices, local(): lax.psum_scatter(jnp.dot(attended, w_out_attn, preferred_element_type=jnp...  24.5 us
    all_gather x1, blocking collectives, local(): lax.all_gather(weights_in[0], 'sp', axis=0, tiled=True)  18.7 us
    all_gather x1, blocking collectives, local(): lax.all_gather(value_rows, 'sp', axis=0, tiled=True)  14.4 us
    all_gather x1, blocking collectives, local(): lax.all_gather(key_rows, 'sp', axis=0, tiled=True)  13.4 us
    all_gather x1, blocking collectives, local(): lax.all_gather(key_offset, 'sp', axis=0, tiled=True)  9.91 us
    all_gather x1, blocking collectives, local(): lax.all_gather(row_norm(share, out_gain).astype(jnp.bfloat16), 'tp', axis...  6.62 us
    all_to_all x1, starting transfers between devices, swapped_in(): shards = lax.all_to_all(shards, axis, split_axis=0, concat_axis=0)  6.48 us
  transfers between devices with their start and end apart: 5, of which 2 were waited for; matrix products, arithmetic and copies ran while one was open for 5% of the time, Pallas kernels for 0%

profile of v1, /device:TPU:0, one launch (start us, length us, event | category | flops | bytes accessed | tf_op | source)
XLA Modules:
  0.0 176.6 jit_solution(10923173160230297773)
XLA Ops:
  7.2 0.0 all-gather.3.cloned.1.call-start
  7.2 0.7 all-gather.3.cloned.1.call-update
  7.9 0.2 copy-done.4
  8.2 0.9 stack.2
  9.0 6.5 %all-to-all-start = ((bf16[4,512,128]{2,1,0:T(8,128)(2,1)}), bf16[4,512,128]{2,1,0:T(8,128)(2,1)S(1)}, u32[]{:S(2)}, u32[]{:S(2)}) async-start(bf16[4,512,128]{2,1,0:T(8,128)(2,1)} %stack.2), calls=%async_computation | async-start | bytes 1048576 | tf_op jit(solution)/shard_map/all_to_all | solution.py:14
  15.5 0.7 all-gather.5.cloned.1.call-update
  16.3 0.0 reduce-scatter.2.cloned.1.call-start
  16.3 0.2 fusion.28
  16.5 0.6 copy-done.5
  17.2 39.7 %all_gather.27 = bf16[2048,128]{1,0:T(8,128)(2,1)S(1)} all-gather(bf16[512,128]{1,0:T(8,128)(2,1)S(1)} %copy-done.5), channel_id=1, replica_groups=mesh['grp'=2,'sp'=4,'tp'=4] {'sp'}, dimensions={0}, use_global_device_ids=true | all-gather | bytes 655360 | tf_op jit(solution)/shard_map/all_gather | solution.py:52
  56.8 0.4 convolution_convert_fusion.2
  57.2 0.5 copy-done.6
  57.7 18.7 %all_gather.24 = bf16[2048,128]{1,0:T(8,128)(2,1)S(1)} all-gather(bf16[512,128]{1,0:T(8,128)(2,1)S(1)} %copy-done.6), channel_id=1, replica_groups=mesh['grp'=2,'sp'=4,'tp'=4] {'sp'}, dimensions={0}, use_global_device_ids=true | all-gather | bytes 655360 | tf_op jit(solution)/shard_map/all_gather | solution.py:50
  76.4 14.4 %all_gather.28 = bf16[512,128]{1,0:T(8,128)(2,1)S(1)} all-gather(bf16[128,128]{1,0:T(8,128)(2,1)S(1)} %convolution_convert_fusion.2), channel_id=1, replica_groups=mesh['grp'=2,'sp'=4,'tp'=4] {'sp'}, dimensions={0}, use_global_device_ids=true | all-gather | bytes 163840 | tf_op jit(solution)/shard_map/all_gather | solution.py:67
  90.8 0.1 copy.28
  91.0 0.7 copy-done.13
  91.6 0.1 mul.427
  91.7 0.6 copy-done.11
  92.3 9.9 %all_gather.26 = bf16[512,2]{0,1:T(2,128)(2,1)S(1)} all-gather(bf16[128,2]{0,1:T(2,128)(2,1)S(1)} %copy-done.11), channel_id=1, replica_groups=mesh['grp'=2,'sp'=4,'tp'=4] {'sp'}, dimensions={0}, use_global_device_ids=true | all-gather | bytes 2560 | tf_op jit(solution)/shard_map/all_gather | solution.py:68
  102.2 0.4 convolution_convert_fusion.4
  102.7 0.4 convolution_convert_fusion.3
  103.0 13.4 %all_gather.25 = bf16[512,128]{1,0:T(8,128)(2,1)S(1)} all-gather(bf16[128,128]{1,0:T(8,128)(2,1)S(1)} %convolution_convert_fusion.3), channel_id=1, replica_groups=mesh['grp'=2,'sp'=4,'tp'=4] {'sp'}, dimensions={0}, use_global_device_ids=true | all-gather | bytes 163840 | tf_op jit(solution)/shard_map/all_gather | solution.py:66
  116.4 0.1 copy.27
  116.6 4.3 %while.15 = (s32[]{:T(128)}, f32[2,1,128,64]{2,3,0,1:T(8,128)S(1)}, f32[2,1,128]{2,1,0:T(1,128)S(1)}, f32[2,1,128]{2,0,1:T(2,128)S(1)}, s32[]{:T(128)}, /*index=...) while((s32[]{:T(128)}, f32[2,1,128,64]{2,3,0,1:T(8,128)S(1)}, ...), condition=%wide.region_6.7_spmd.clone, body=%wide.region_1.6_spmd.clone.sunk | while | flops 54744452 | bytes 5395625 | solution.py:116
  116.6 0.1 broadcast_compare_fusion.2
  116.8 0.6 fusion.104
  117.4 2.4 %fusion.105 = f32[2,1,128,4,128]{2,3,4,1,0:T(4,128)S(1)} fusion(f32[2,1,128,4,128]{2,4,3,0,1:T(8,128)S(1)} %bitcast.129), kind=kOutput, calls=%fused_computation.18.clone.1 | output fusion | flops 16646144 | bytes 1048576 | tf_op jit(solution)/shard_map/reduce-window
  119.8 0.8 fusion.106
  120.7 0.2 fusion.107
  120.9 0.0 all-gather.3.cloned.1.call-done
  120.9 1.6 fusion.27
  122.5 0.0 all-gather.5.cloned.1.call-done
  122.5 1.6 fusion.26
  124.2 1.3 collective-permute-start
  125.5 0.1 fusion.63
  125.6 1.3 collective-permute-done
  126.9 0.6 fusion.76
  127.5 5.8 %all-reduce = (f32[128]{0:T(128)S(1)}, f32[128]{0:T(128)S(1)}) all-reduce(f32[128]{0:T(128)S(1)} %get-tuple-element.112, f32[128]{0:T(128)S(1)} %get-tuple-element.111), channel_id=1, replica_groups=mesh['grp'=2,'sp'=4,'tp'=4] {'tp'}, use_global_device_ids=true, to_apply=%region_11.12 | all-reduce | flops 256 | bytes 2048 | tf_op jit(solution)/shard_map/psum | solution.py:133
  133.3 0.7 copy-done.9
  133.9 0.4 fusion.61
  134.3 0.7 copy-done.3
  135.0 1.3 convolution_add_fusion
  136.3 0.6 log_bitcast_fusion
  136.9 24.5 %reduce-scatter.2.cloned.1.call-done = f32[32,2048]{1,0:T(8,128)} async-done(((f32[128,2048]{1,0:T(8,128)}), f32[32,2048]{1,0:T(8,128)}) %reduce-scatter.2.cloned.1.call-update) | async-done | bytes 262160 | tf_op jit(solution)/shard_map/reduce_scatter | solution.py:142
  161.4 1.1 multiply_reduce_fusion
  162.6 0.1 multiply_convert_fusion
  162.6 6.6 %all_gather.31 = bf16[128,2048]{1,0:T(8,128)(2,1)S(1)} all-gather(bf16[32,2048]{1,0:T(8,128)(2,1)S(1)} %multiply_convert_fusion), channel_id=1, replica_groups=mesh['grp'=2,'sp'=4,'tp'=4] {'tp'}, dimensions={0}, use_global_device_ids=true | all-gather | bytes 655360 | tf_op jit(solution)/shard_map/all_gather | solution.py:149
  169.3 0.8 copy.53
  (45 shorter events, 0.3 us)
Async XLA Ops:
  7.2 126.1 %copy-start = (bf16[256,2048]{1,0:T(8,128)(2,1)S(1)}, bf16[256,2048]{1,0:T(8,128)(2,1)}, u32[]{:S(2)}) copy-start(bf16[256,2048]{1,0:T(8,128)(2,1)} %param.30) | copy-start | bytes 3145732
  7.2 1.0 copy-start.4
  7.2 113.7 %all-gather.3.cloned.1.call-start = ((), (), s32[]{:S(2)}) async-start(), calls=%async_computation.2 | async-start | bytes 1310720 | tf_op jit(solution)/shard_map/all_gather | solution.py:53
  9.0 7.3 %copy-start.2 = (bf16[128,2048]{1,0:T(8,128)(2,1)S(1)}, bf16[128,2048]{1,0:T(8,128)(2,1)}, u32[]{:S(2)}) copy-start(bf16[128,2048]{1,0:T(8,128)(2,1)} %param.17) | copy-start | bytes 1572868
  9.0 93.6 %all-to-all-start = ((bf16[4,512,128]{2,1,0:T(8,128)(2,1)}), bf16[4,512,128]{2,1,0:T(8,128)(2,1)S(1)}, u32[]{:S(2)}, u32[]{:S(2)}) async-start(bf16[4,512,128]{2,1,0:T(8,128)(2,1)} %stack.2), calls=%async_computation | async-start | bytes 1048576 | tf_op jit(solution)/shard_map/all_to_all | solution.py:14
  15.5 107.0 %all-gather.5.cloned.1.call-start = ((), (), s32[]{:S(2)}) async-start(), calls=%async_computation.3 | async-start | bytes 1310720 | tf_op jit(solution)/shard_map/all_gather | solution.py:54
  16.2 0.9 copy-start.5
  16.3 145.1 %reduce-scatter.2.cloned.1.call-start = ((), (), s32[]{:S(2)}) async-start(), calls=%async_computation.4 | async-start | bytes 1310720 | tf_op jit(solution)/shard_map/reduce_scatter | solution.py:142
  17.2 39.7 %copy-start.12 = (f32[2048]{0:T(1024)S(1)}, f32[2048]{0:T(1024)}, u32[]{:S(2)}) copy-start(f32[2048]{0:T(1024)} %param.18) | copy-start | bytes 24580
  56.8 0.9 copy-start.6
  90.8 11.4 %copy-start.7 = (f32[31,256]{1,0:T(8,128)S(1)}, f32[31,256]{1,0:T(8,128)}, u32[]{:S(2)}) copy-start(f32[31,256]{1,0:T(8,128)} %param.26) | copy-start | bytes 95236
  90.9 0.7 copy-start.13
  91.6 0.7 copy-start.11
  124.2 2.7 %collective-permute-start = (bf16[30,256]{1,0:T(8,128)(2,1)S(1)}, bf16[30,256]{1,0:T(8,128)(2,1)S(1)}, u32[]{:S(2)}, u32[]{:S(2)}) collective-permute-start(bf16[30,256]{1,0:T(8,128)(2,1)S(1)} %slice.262), channel_id=1, source_target_pairs={{0,4},{4,8},{8,12},{1,5},{5,9},{9,13},{2,6},{6,10},{10,14},{3,7},{... | collective-permute-start | bytes 46088 | tf_op jit(solution)/shard_map/ppermute | solution.py:21
  126.9 6.4 %copy-start.10 = (f32[256]{0:T(256)S(1)}, f32[256]{0:T(256)}, u32[]{:S(2)}) copy-start(f32[256]{0:T(256)} %param.27) | copy-start | bytes 3076
  133.3 0.7 copy-start.9
  133.9 1.0 copy-start.3
  136.3 26.2 %copy-start.8 = (f32[2048]{0:T(1024)S(1)}, f32[2048]{0:T(1024)}, u32[]{:S(2)}) copy-start(f32[2048]{0:T(1024)} %param.31) | copy-start | bytes 24580
  161.4 1.2 copy-start.1
Sparse Core Ops, SparseCore 0:
  9.6 45.3 all-gather.2
  56.6 31.2 all-gather.4
  136.4 24.8 reduce-scatter.1
